TPU v7x, 256 devices: a 4x2x16 block of a 4x16x16 slice. The times are simulated.
256 devices in a mesh: grp: 2 (over y), fs: 32 (over z, core), tp: 4 (over x).
Axes of the slice: x: 4, y: 2, z: 16, core: 2. Of those that a mesh axis runs over, the one named last changes fastest.
The devices are a block of a 4x16x16 slice.
Arguments:
- prompt: bfloat16 [8, 1024, 2048], P(('grp', 'tp')), parts along dimension 0, may hold values from -6 to 6
- gate_first: float32 [2048, 5632], P('fs', 'tp'), may hold values from -0.125 to 0.125
- up_first: float32 [2048, 5632], P('fs', 'tp'), may hold values from -0.125 to 0.125
- down_first: float32 [5632, 2048], P('fs', 'tp'), may hold values from -0.3125 to 0.3125
- norm_gain: float32 [2048], replicated, may hold values from 0.1 to 1.9
- gate_second: float32 [2048, 5632], P('fs', 'tp'), may hold values from -0.125 to 0.125
- up_second: float32 [2048, 5632], P('fs', 'tp'), may hold values from -0.125 to 0.125
- down_second: float32 [5632, 2048], P('fs', 'tp'), may hold values from -0.3125 to 0.3125
Outputs:
- result: bfloat16 [8, 1024, 2048], P(('grp', 'tp'), 'fs'), parts along dimension 0
- gate_one: bfloat16 [4096, 5632], P('grp', 'fs'), parts along dimension 0
- up_one: bfloat16 [4096, 5632], P('grp', 'fs'), parts along dimension 0
- down_one: bfloat16 [5632, 4096], P('fs', 'grp'), parts along dimension 1
- gate_two: bfloat16 [4096, 5632], P('grp', 'fs'), parts along dimension 0
- up_two: bfloat16 [4096, 5632], P('grp', 'fs'), parts along dimension 0
- down_two: bfloat16 [5632, 4096], P('fs', 'grp'), parts along dimension 1
There are 2 independent parts, one for each index of `grp`. A program takes and returns all parts, laid end to end along the dimension named above; an argument that names none is the same for every part. Nothing has to cross between parts.
All inputs are finite; a program needn't handle non-finite values.
Results may differ from a plain program's by a relative error of at most 0.029.
Values may be sent and summed in bfloat16 or wider, within the bound.
A program may use at most 64 MiB of HBM per device.

v0:
```python
import jax
import jax.numpy as jnp
from jax import lax
from jax.sharding import Mesh
from jax.sharding import PartitionSpec as P

FS = ("fs_0", "fs_1")
norm_eps = 1e-05
deep_alpha = 2.0**0.25
half_step = 0.5


def reduced_to_own(pieces, axes, sequence):
    inside = pieces.shape[1:]
    pieces = pieces.reshape(*(lax.axis_size(a) for a in axes), *inside)
    pieces = jnp.moveaxis(pieces, sequence, range(len(axes))).reshape(-1, *inside)
    for k in sequence:
        pieces = lax.psum_scatter(pieces, axes[k], scatter_dimension=0, tiled=True)
    return pieces[0]


def cut_along(value, dim, size):
    before, after = (value.shape[:dim], value.shape[dim + 1 :])
    return jnp.moveaxis(value.reshape(*before, size, -1, *after), dim, 0)


def scatter_axes(value, axes, sequence, dim):
    size = lax.axis_size(axes)
    return reduced_to_own(cut_along(value, dim, size), axes, sequence)


def plain_norm(values):
    row_mean = jnp.mean(values, axis=-1, keepdims=True)
    centred = values - row_mean
    variance = jnp.mean(centred * centred, axis=-1, keepdims=True)
    return centred * lax.rsqrt(variance + norm_eps)


def gated_hidden(inputs, gate_proj, up_proj):
    gate_act = jnp.dot(inputs, gate_proj, preferred_element_type=jnp.float32)
    up_act = jnp.dot(inputs, up_proj, preferred_element_type=jnp.float32)
    return (jax.nn.silu(gate_act) * up_act).astype(jnp.bfloat16)


def relay_weights(gate_proj, up_proj, down_proj):
    gate_rows, up_rows, down_mine = (
        lax.all_gather(gate_proj, "tp", axis=1, tiled=True),
        lax.all_gather(up_proj, "tp", axis=1, tiled=True),
        lax.all_gather(down_proj, "tp", axis=1, tiled=True),
    )
    gate_mine, up_mine = (
        lax.all_to_all(gate_rows, FS, split_axis=1, concat_axis=0, tiled=True),
        lax.all_to_all(up_rows, FS, split_axis=1, concat_axis=0, tiled=True),
    )
    return (gate_mine, up_mine, down_mine)


def row_terms(hidden, down_proj):
    return jnp.dot(hidden, down_proj, preferred_element_type=jnp.float32)


def body(prompt, gate_first, up_first, down_first, norm_gain, gate_second, up_second, down_second):
    fs_index = lax.axis_index(FS)
    row_block = gate_first.shape[0]
    gain_rows = lax.dynamic_slice_in_dim(norm_gain, fs_index * row_block, row_block, 0)
    gate_one, up_one, down_one = relay_weights(
        gate_first.astype(jnp.bfloat16),
        up_first.astype(jnp.bfloat16),
        down_first.astype(jnp.bfloat16),
    )
    gate_two, up_two, down_two = relay_weights(
        (gain_rows[:, None] * gate_second).astype(jnp.bfloat16),
        (gain_rows[:, None] * up_second).astype(jnp.bfloat16),
        down_second.astype(jnp.bfloat16),
    )
    tokens = prompt.reshape(-1, prompt.shape[-1])
    own_count = tokens.shape[0] // lax.axis_size(FS)
    own_first = fs_index * own_count
    hidden_one = gated_hidden(tokens, gate_one, up_one)
    own_tokens = lax.dynamic_slice_in_dim(tokens, own_first, own_count, 0)
    ffn_one = scatter_axes(
        row_terms(hidden_one, down_one).astype(jnp.bfloat16), FS, (1, 0), 0
    ).astype(jnp.float32)
    normed_own = plain_norm(
        deep_alpha * own_tokens.astype(jnp.float32) + half_step * ffn_one
    ).astype(jnp.bfloat16)
    hidden_two = gated_hidden(lax.all_gather(normed_own, FS, axis=0, tiled=True), gate_two, up_two)
    ffn_two = scatter_axes(
        row_terms(hidden_two, down_two).astype(jnp.bfloat16), FS, (1, 0), 0
    ).astype(jnp.float32)
    residual_two = deep_alpha * norm_gain * normed_own.astype(jnp.float32)
    result = plain_norm(residual_two + half_step * ffn_two).astype(jnp.bfloat16)
    return (
        result.reshape(1, result.shape[0], result.shape[-1]),
        gate_one,
        up_one,
        down_one,
        gate_two,
        up_two,
        down_two,
    )


def solution(mesh):
    torus = Mesh(
        mesh.devices.reshape(mesh.shape["grp"], 16, 2, mesh.shape["tp"]),
        ("grp", "fs_0", "fs_1", "tp"),
    )
    placed = (
        P(("grp", "tp"), None, None),
        P(FS, "tp"),
        P(FS, "tp"),
        P(FS, "tp"),
        P(),
        P(FS, "tp"),
        P(FS, "tp"),
        P(FS, "tp"),
    )
    return jax.shard_map(
        body,
        mesh=torus,
        in_specs=placed,
        out_specs=(
            P(("grp", "tp"), FS, None),
            P("grp", FS),
            P("grp", FS),
            P(FS, "grp"),
            P("grp", FS),
            P("grp", FS),
            P(FS, "grp"),
        ),
        check_vma=False,
    )
```

profile of v0, /device:TPU:34, one launch (start us, length us, event | category | flops | bytes accessed | tf_op | source)
XLA Modules:
  0.0 540.0 jit_solution(11706451847986128299)
XLA Ops:
  7.2 0.0 copy-start.3
  7.2 1.1 convert_element_type.62
  8.2 29.5 %all_gather.21 = bf16[64,5632]{1,0:T(8,128)(2,1)S(1)} all-gather(bf16[64,1408]{1,0:T(8,128)(2,1)S(1)} %convert_element_type.62), channel_id=1, replica_groups=mesh['grp'=2,'fs_0'=16,'fs_1'=2,'tp'=4] {'tp'}, dimensions={1}, use_global_device_ids=true | all-gather | bytes 901120 | tf_op jit(solution)/shard_map/all_gather | solution.py:47
  37.8 2.0 all_to_all.56
  39.8 1.6 copy.21
  41.4 9.7 %all-to-all-start = ((bf16[64,32,176]{2,0,1:T(8,128)(2,1)}), bf16[64,32,176]{2,0,1:T(8,128)(2,1)S(1)}, u32[]{:S(2)}, u32[]{:S(2)}) async-start(bf16[64,32,176]{2,0,1:T(8,128)(2,1)} %copy.21), calls=%async_computation | async-start | bytes 2097152 | tf_op jit(solution)/shard_map/all_to_all | solution.py:52
  51.1 0.0 copy-done.3
  51.1 0.0 copy-start.4
  51.2 14.4 %all_gather.22 = bf16[64,5632]{1,0:T(8,128)(2,1)S(1)} all-gather(bf16[64,1408]{1,0:T(8,128)(2,1)S(1)} %convert_element_type.63), channel_id=1, replica_groups=mesh['grp'=2,'fs_0'=16,'fs_1'=2,'tp'=4] {'tp'}, dimensions={1}, use_global_device_ids=true | all-gather | bytes 901120 | tf_op jit(solution)/shard_map/all_gather | solution.py:48
  65.5 2.0 all_to_all.60
  67.6 1.5 copy.22
  69.1 37.3 %all-to-all-done = bf16[64,32,176]{2,0,1:T(8,128)(2,1)S(1)} async-done(((bf16[64,32,176]{2,0,1:T(8,128)(2,1)}), bf16[64,32,176]{2,0,1:T(8,128)(2,1)S(1)}, u32[]{:S(2)}, u32[]{:S(2)}) %all-to-all-start) | async-done | bytes 720928 | tf_op jit(solution)/shard_map/all_to_all | solution.py:52
  106.4 4.8 all-to-all-start.1
  111.3 0.1 reduce-scatter.5.cloned.1.call-start
  111.3 0.0 copy-done.4
  111.4 14.2 %all_gather.23 = bf16[176,2048]{1,0:T(8,128)(2,1)S(1)} all-gather(bf16[176,512]{1,0:T(8,128)(2,1)S(1)} %convert_element_type.65), channel_id=1, replica_groups=mesh['grp'=2,'fs_0'=16,'fs_1'=2,'tp'=4] {'tp'}, dimensions={1}, use_global_device_ids=true | all-gather | bytes 901120 | tf_op jit(solution)/shard_map/all_gather | solution.py:49
  125.6 4.0 fusion.2
  129.6 37.3 %all-to-all-done.1 = bf16[64,32,176]{2,0,1:T(8,128)(2,1)S(1)} async-done(((bf16[64,32,176]{2,0,1:T(8,128)(2,1)}), bf16[64,32,176]{2,0,1:T(8,128)(2,1)S(1)}, u32[]{:S(2)}, u32[]{:S(2)}) %all-to-all-start.1) | async-done | bytes 720928 | tf_op jit(solution)/shard_map/all_to_all | solution.py:53
  167.0 7.0 %convolution_convert_fusion.1 = bf16[1024,2048]{1,0:T(8,128)(2,1)} fusion(bf16[176,2048]{1,0:T(8,128)(2,1)S(1)} %all_gather.23, bf16[2048,176]{1,0:T(8,128)(2,1)S(1)} %bitcast.57, bf16[1,1024,2048]{2,1,0:T(8,128)(2,1)} %param.8, f32[1024,176]{0,1:T(8,128)S(1)} %fusion.2), kind=kOutput, calls=%fused_computation.5 | convolution fusion | flops 1479573504 | bytes 10551296 | tf_op jit(solution)/shard_map/dot_general | solution.py:59
  173.9 4.7 copy.23
  178.7 0.1 reduce-scatter.5.cloned.1.call-update
  178.7 0.1 reduce-scatter.7.cloned.1.call-start
  178.8 12.5 %reduce-scatter.5.cloned.1.call-done = bf16[16,32,2048]{2,1,0:T(8,128)(2,1)} async-done(((bf16[32,32,2048]{2,1,0:T(8,128)(2,1)}), bf16[16,32,2048]{2,1,0:T(8,128)(2,1)}) %reduce-scatter.5.cloned.1.call-update) | async-done | bytes 2097168 | tf_op jit(solution)/shard_map/reduce_scatter | solution.py:18
  191.3 0.1 reduce-scatter.7.cloned.1.call-update
  191.3 0.1 all-gather.2.cloned.1.call-start
  191.4 75.9 %reduce-scatter.7.cloned.1.call-done = bf16[1,32,2048]{2,1,0:T(8,128)(2,1)} async-done(((bf16[16,32,2048]{2,1,0:T(8,128)(2,1)}), bf16[1,32,2048]{2,1,0:T(8,128)(2,1)}) %reduce-scatter.7.cloned.1.call-update) | async-done | bytes 131088 | tf_op jit(solution)/shard_map/reduce_scatter | solution.py:18
  267.4 1.1 fusion.26
  268.5 1.2 multiply_reduce_fusion.1
  269.7 1.7 multiply_convert_fusion.3
  271.4 0.1 all-gather.2.cloned.1.call-update
  271.5 0.0 copy-done.8
  271.5 0.1 dynamic_slice.7
  271.6 0.0 copy-done.6
  271.6 0.1 multiply_convert_fusion.1
  271.7 14.1 %all_gather.25 = bf16[64,5632]{1,0:T(8,128)(2,1)} all-gather(bf16[64,1408]{1,0:T(8,128)(2,1)S(1)} %get-tuple-element.14), channel_id=1, replica_groups=mesh['grp'=2,'fs_0'=16,'fs_1'=2,'tp'=4] {'tp'}, dimensions={1}, use_global_device_ids=true | all-gather | bytes 901120 | tf_op jit(solution)/shard_map/all_gather | solution.py:47
  285.8 3.0 all_to_all.64
  288.8 1.5 copy.24
  290.4 9.7 %all-to-all-start.2 = ((bf16[64,32,176]{2,0,1:T(8,128)(2,1)}), bf16[64,32,176]{2,0,1:T(8,128)(2,1)S(1)}, u32[]{:S(2)}, u32[]{:S(2)}) async-start(bf16[64,32,176]{2,0,1:T(8,128)(2,1)} %copy.24), calls=%async_computation.4 | async-start | bytes 2097152 | tf_op jit(solution)/shard_map/all_to_all | solution.py:52
  300.1 14.3 %all_gather.26 = bf16[64,5632]{1,0:T(8,128)(2,1)} all-gather(bf16[64,1408]{1,0:T(8,128)(2,1)S(1)} %get-tuple-element.15), channel_id=1, replica_groups=mesh['grp'=2,'fs_0'=16,'fs_1'=2,'tp'=4] {'tp'}, dimensions={1}, use_global_device_ids=true | all-gather | bytes 901120 | tf_op jit(solution)/shard_map/all_gather | solution.py:48
  314.4 3.8 all_to_all.68
  318.2 2.8 copy.25
  321.0 44.7 %all-to-all-done.2 = bf16[64,32,176]{2,0,1:T(8,128)(2,1)S(1)} async-done(((bf16[64,32,176]{2,0,1:T(8,128)(2,1)}), bf16[64,32,176]{2,0,1:T(8,128)(2,1)S(1)}, u32[]{:S(2)}, u32[]{:S(2)}) %all-to-all-start.2) | async-done | bytes 720928 | tf_op jit(solution)/shard_map/all_to_all | solution.py:52
  365.7 5.7 %all-to-all-start.3 = ((bf16[64,32,176]{2,0,1:T(8,128)(2,1)}), bf16[64,32,176]{2,0,1:T(8,128)(2,1)}, u32[]{:S(2)}, u32[]{:S(2)}) async-start(bf16[64,32,176]{2,0,1:T(8,128)(2,1)} %copy.25), calls=%async_computation.5 | async-start | bytes 2097152 | tf_op jit(solution)/shard_map/all_to_all | solution.py:53
  371.4 0.1 reduce-scatter.9.cloned.1.call-start
  371.5 14.5 %all_gather.27 = bf16[176,2048]{1,0:T(8,128)(2,1)} all-gather(bf16[176,512]{1,0:T(8,128)(2,1)S(1)} %convert_element_type.74), channel_id=1, replica_groups=mesh['grp'=2,'fs_0'=16,'fs_1'=2,'tp'=4] {'tp'}, dimensions={1}, use_global_device_ids=true | all-gather | bytes 901120 | tf_op jit(solution)/shard_map/all_gather | solution.py:49
  386.0 4.6 fusion.29
  390.6 36.6 %all-to-all-done.3 = bf16[64,32,176]{2,0,1:T(8,128)(2,1)} async-done(((bf16[64,32,176]{2,0,1:T(8,128)(2,1)}), bf16[64,32,176]{2,0,1:T(8,128)(2,1)}, u32[]{:S(2)}, u32[]{:S(2)}) %all-to-all-start.3) | async-done | bytes 720928 | tf_op jit(solution)/shard_map/all_to_all | solution.py:53
  427.2 7.7 %convolution_convert_fusion = bf16[1024,2048]{1,0:T(8,128)(2,1)} fusion(bf16[176,2048]{1,0:T(8,128)(2,1)} %all_gather.27, bf16[1024,2048]{1,0:T(8,128)(2,1)} %all-gather.2.cloned.1.call-done, bf16[2048,176]{1,0:T(8,128)(2,1)} %bitcast.12, f32[1024,176]{0,1:T(8,128)} %fusion.29), kind=kOutput, calls=%fused_computation.4 | convolution fusion | flops 1479573504 | bytes 10551296 | tf_op jit(solution)/shard_map/dot_general | solution.py:59
  434.9 4.7 copy.26
  439.6 0.1 reduce-scatter.9.cloned.1.call-update
  439.7 0.1 reduce-scatter.11.cloned.1.call-start
  439.7 11.8 %reduce-scatter.9.cloned.1.call-done = bf16[16,32,2048]{2,1,0:T(8,128)(2,1)} async-done(((bf16[32,32,2048]{2,1,0:T(8,128)(2,1)}), bf16[16,32,2048]{2,1,0:T(8,128)(2,1)}) %reduce-scatter.9.cloned.1.call-update) | async-done | bytes 2097168 | tf_op jit(solution)/shard_map/reduce_scatter | solution.py:18
  451.6 0.1 reduce-scatter.11.cloned.1.call-update
  451.6 1.2 copy.29
  452.9 2.3 copy.30
  455.1 1.2 copy.27
  456.3 1.2 copy.28
  457.6 70.1 %reduce-scatter.11.cloned.1.call-done = bf16[1,32,2048]{2,1,0:T(8,128)(2,1)} async-done(((bf16[16,32,2048]{2,1,0:T(8,128)(2,1)}), bf16[1,32,2048]{2,1,0:T(8,128)(2,1)}) %reduce-scatter.11.cloned.1.call-update) | async-done | bytes 131088 | tf_op jit(solution)/shard_map/reduce_scatter | solution.py:18
  527.6 1.1 fusion.25
  528.7 1.2 multiply_reduce_fusion
  529.9 1.9 multiply_convert_fusion.2
  531.8 0.0 copy-done.1
  531.8 0.9 copy.33
  532.6 0.9 copy.34
  (20 shorter events, 0.1 us)
Async XLA Ops:
  7.2 43.9 %copy-start.3 = (f32[64,1408]{1,0:T(8,128)S(1)}, f32[64,1408]{1,0:T(8,128)}, u32[]{:S(2)}) copy-start(f32[64,1408]{1,0:T(8,128)} %param.10) | copy-start | bytes 1081348
  41.4 65.0 %all-to-all-start = ((bf16[64,32,176]{2,0,1:T(8,128)(2,1)}), bf16[64,32,176]{2,0,1:T(8,128)(2,1)S(1)}, u32[]{:S(2)}, u32[]{:S(2)}) async-start(bf16[64,32,176]{2,0,1:T(8,128)(2,1)} %copy.21), calls=%async_computation | async-start | bytes 2097152 | tf_op jit(solution)/shard_map/all_to_all | solution.py:52
  51.1 60.2 %copy-start.4 = (f32[176,512]{1,0:T(8,128)S(1)}, f32[176,512]{1,0:T(8,128)}, u32[]{:S(2)}) copy-start(f32[176,512]{1,0:T(8,128)} %param.11) | copy-start | bytes 1081348
  106.4 60.6 %all-to-all-start.1 = ((bf16[64,32,176]{2,0,1:T(8,128)(2,1)}), bf16[64,32,176]{2,0,1:T(8,128)(2,1)S(1)}, u32[]{:S(2)}, u32[]{:S(2)}) async-start(bf16[64,32,176]{2,0,1:T(8,128)(2,1)} %copy.22), calls=%async_computation.1 | async-start | bytes 2097152 | tf_op jit(solution)/shard_map/all_to_all | solution.py:53
  111.3 80.0 %reduce-scatter.5.cloned.1.call-start = ((), (), s32[]{:S(2)}) async-start(), calls=%async_computation.8 | async-start | bytes 6291456 | tf_op jit(solution)/shard_map/reduce_scatter | solution.py:18
  125.6 41.4 %copy-start = (bf16[176,2048]{1,0:T(8,128)(2,1)}, bf16[176,2048]{1,0:T(8,128)(2,1)S(1)}, u32[]{:S(2)}) copy-start(bf16[176,2048]{1,0:T(8,128)(2,1)S(1)} %all_gather.23) | copy-start | bytes 2162692
  178.7 92.8 %copy-start.8 = (f32[2048]{0:T(1024)S(1)}, f32[2048]{0:T(1024)}, u32[]{:S(2)}) copy-start(f32[2048]{0:T(1024)} %param.12) | copy-start | bytes 24580
  178.7 92.9 %copy-start.6 = (f32[64,1408]{1,0:T(8,128)S(1)}, f32[64,1408]{1,0:T(8,128)}, u32[]{:S(2)}) copy-start(f32[64,1408]{1,0:T(8,128)} %param.13) | copy-start | bytes 1081348
  178.7 92.9 %copy-start.7 = (f32[64,1408]{1,0:T(8,128)S(1)}, f32[64,1408]{1,0:T(8,128)}, u32[]{:S(2)}) copy-start(f32[64,1408]{1,0:T(8,128)} %param.14) | copy-start | bytes 1081348
  178.7 88.6 %reduce-scatter.7.cloned.1.call-start = ((), (), s32[]{:S(2)}) async-start(), calls=%async_computation.9 | async-start | bytes 2228224 | tf_op jit(solution)/shard_map/reduce_scatter | solution.py:18
  191.3 194.7 %all-gather.2.cloned.1.call-start = ((), (), s32[]{:S(2)}) async-start(), calls=%async_computation.10 | async-start | bytes 4325376 | tf_op jit(solution)/shard_map/all_gather | solution.py:87
  290.4 75.3 %all-to-all-start.2 = ((bf16[64,32,176]{2,0,1:T(8,128)(2,1)}), bf16[64,32,176]{2,0,1:T(8,128)(2,1)S(1)}, u32[]{:S(2)}, u32[]{:S(2)}) async-start(bf16[64,32,176]{2,0,1:T(8,128)(2,1)} %copy.24), calls=%async_computation.4 | async-start | bytes 2097152 | tf_op jit(solution)/shard_map/all_to_all | solution.py:52
  314.4 57.1 %copy-start.5 = (f32[176,512]{1,0:T(8,128)S(1)}, f32[176,512]{1,0:T(8,128)}, u32[]{:S(2)}) copy-start(f32[176,512]{1,0:T(8,128)} %param.15) | copy-start | bytes 1081348
  365.7 61.5 %all-to-all-start.3 = ((bf16[64,32,176]{2,0,1:T(8,128)(2,1)}), bf16[64,32,176]{2,0,1:T(8,128)(2,1)}, u32[]{:S(2)}, u32[]{:S(2)}) async-start(bf16[64,32,176]{2,0,1:T(8,128)(2,1)} %copy.25), calls=%async_computation.5 | async-start | bytes 2097152 | tf_op jit(solution)/shard_map/all_to_all | solution.py:53
  371.4 80.1 %reduce-scatter.9.cloned.1.call-start = ((), (), s32[]{:S(2)}) async-start(), calls=%async_computation.11 | async-start | bytes 6291456 | tf_op jit(solution)/shard_map/reduce_scatter | solution.py:18
  439.7 87.9 %reduce-scatter.11.cloned.1.call-start = ((), (), s32[]{:S(2)}) async-start(), calls=%async_computation.12 | async-start | bytes 2228224 | tf_op jit(solution)/shard_map/reduce_scatter | solution.py:18
  452.9 78.9 %copy-start.1 = (bf16[176,2048]{1,0:T(8,128)(2,1)S(1)}, bf16[176,2048]{1,0:T(8,128)(2,1)}, u32[]{:S(2)}) copy-start(bf16[176,2048]{1,0:T(8,128)(2,1)} %copy-done) | copy-start | bytes 2162692
  452.9 79.8 %copy-start.2 = (bf16[176,2048]{1,0:T(8,128)(2,1)S(1)}, bf16[176,2048]{1,0:T(8,128)(2,1)}, u32[]{:S(2)}) copy-start(bf16[176,2048]{1,0:T(8,128)(2,1)} %all_gather.27) | copy-start | bytes 2162692
Sparse Core Ops, SparseCore 0:
  178.9 12.3 reduce-scatter.4
  193.8 73.4 reduce-scatter.6
  271.6 98.2 all-gather.1
  439.8 11.7 reduce-scatter.8
  454.0 73.5 reduce-scatter.10
where the time goes:
time: 541 us; the launch traced here: 540 us
  waiting for transfers between devices  326 us (60%)
  blocking collectives  101 us (19%)
  local copies, waits for them, and re-layouts  35.6 us (7%)
  starting transfers between devices  30.2 us (6%)
  matrix products  23.2 us (4%)
  between operations  14 us (3%)
  other arithmetic  9.45 us (2%)
    reduce_scatter x4, waiting for transfers between devices, reduced_to_own(): pieces = lax.psum_scatter(pieces, axes[k], scatter_dimension=0, tiled=True)  170 us
    all_to_all x2, waiting for transfers between devices, relay_weights(): lax.all_to_all(gate_rows, FS, split_axis=1, concat_axis=0, tiled=True)  82 us
    all_to_all x2, waiting for transfers between devices, relay_weights(): lax.all_to_all(up_rows, FS, split_axis=1, concat_axis=0, tiled=True)  73.9 us
    all_gather x2, blocking collectives, relay_weights(): lax.all_gather(gate_proj, 'tp', axis=1, tiled=True)  43.7 us
    all_gather x2, blocking collectives, relay_weights(): lax.all_gather(down_proj, 'tp', axis=1, tiled=True)  28.7 us
    all_gather x2, blocking collectives, relay_weights(): lax.all_gather(up_proj, 'tp', axis=1, tiled=True)  28.6 us
    all_to_all x2, starting transfers between devices, relay_weights(): lax.all_to_all(gate_rows, FS, split_axis=1, concat_axis=0, tiled=True)  19.4 us
    dot_general x2, matrix products, row_terms(): return jnp.dot(hidden, down_proj, preferred_element_type=jnp.float32)  14.6 us
  transfers between devices with their start and end apart: 9, of which 8 were waited for; matrix products, arithmetic and copies ran while one was open for 4% of the time, Pallas kernels for 0%

commit v1 on v0

--- a/solution.py
+++ b/solution.py
@@ -8,6 +8,32 @@
 norm_eps = 1e-05
 deep_alpha = 2.0**0.25
 half_step = 0.5
+
+
+def track_pipes(state, k_dim):
+    o_now = list(state.shape[1:])
+    o_now[k_dim] *= state.shape[0]
+    return jnp.moveaxis(state, 0, k_dim).reshape(o_now)
+
+
+def arrange_the_seats_all(which_axis, ndim_at, xin):
+    dev_n = lax.axis_size(which_axis)
+    line_up = [(kk, (kk + 1) % dev_n) for kk in range(dev_n)]
+    gallery = [(k0, ii) for ii, k0 in line_up]
+    earlier, val2 = ([], [])
+    for dev_j in [*range(dev_n - 1)]:
+        if dev_j % 2 == 0:
+            later = lax.ppermute(
+                earlier[-1] if earlier else xin, axis_name=which_axis, perm=line_up
+            )
+            earlier.append(later)
+        else:
+            val2.append(lax.ppermute(val2[-1] if val2 else xin, axis_name=which_axis, perm=gallery))
+    tile_out = jnp.stack([*earlier[::-1], xin, *val2])
+    known = lax.axis_index(which_axis)
+    block_now = known - len(earlier)
+    tile_out = tile_out[(jnp.arange(dev_n) - block_now) % dev_n]
+    return track_pipes(tile_out, ndim_at)
 
 
 def reduced_to_own(pieces, axes, sequence):
@@ -44,7 +70,7 @@
 
 def relay_weights(gate_proj, up_proj, down_proj):
     gate_rows, up_rows, down_mine = (
-        lax.all_gather(gate_proj, "tp", axis=1, tiled=True),
+        arrange_the_seats_all("tp", 1, gate_proj),
         lax.all_gather(up_proj, "tp", axis=1, tiled=True),
         lax.all_gather(down_proj, "tp", axis=1, tiled=True),
     )

time: 541 us -> 539 us (level)
  blocking collectives: 101 us -> 56.8 us
  starting transfers between devices: 30.2 us -> 50.8 us
  waiting for transfers between devices: 326 us -> 344 us
    all_gather x2 -> x0, blocking collectives: 43.7 us -> none  [relay_weights(): lax.all_gather(gate_proj, 'tp', axis=1, tiled=True)]
    ppermute x0 -> x6, starting transfers between devices: none -> 23.1 us  [the longest x2 18.5 us: arrange_the_seats_all(): lax.ppermute(val2[-1] if val2 else xin, axis_name=which_axis, perm=gallery)]
    ppermute x0 -> x6, waiting for transfers between devices: none -> 16.5 us  [the longest x4 16.5 us: arrange_the_seats_all(): lax.ppermute(earlier[-1] if earlier else xin, axis_name=which_axis, perm=...]
  transfers between devices with their start and end apart: 9 -> 15, of which waited for: 8 -> 12; matrix products, arithmetic and copies ran while one was open for 4% -> 5% of each run, Pallas kernels for 0% -> 0%
where the time goes in v1:
time: 539 us; the launch traced here: 538 us
  waiting for transfers between devices  344 us (64%)
  blocking collectives  56.8 us (11%)
  starting transfers between devices  50.8 us (9%)
  local copies, waits for them, and re-layouts  38.1 us (7%)
  matrix products  23.2 us (4%)
  between operations  14.1 us (3%)
  other arithmetic  11.1 us (2%)
    reduce_scatter x4, waiting for transfers between devices, reduced_to_own(): pieces = lax.psum_scatter(pieces, axes[k], scatter_dimension=0, tiled=True)  172 us
    all_to_all x2, waiting for transfers between devices, relay_weights(): lax.all_to_all(gate_rows, FS, split_axis=1, concat_axis=0, tiled=True)  81.1 us
    all_to_all x2, waiting for transfers between devices, relay_weights(): lax.all_to_all(up_rows, FS, split_axis=1, concat_axis=0, tiled=True)  73.8 us
    all_gather x2, blocking collectives, relay_weights(): lax.all_gather(down_proj, 'tp', axis=1, tiled=True)  28.4 us
    all_gather x2, blocking collectives, relay_weights(): lax.all_gather(up_proj, 'tp', axis=1, tiled=True)  28.4 us
    ppermute x2, starting transfers between devices, arrange_the_seats_all(): lax.ppermute(val2[-1] if val2 else xin, axis_name=which_axis, perm=gallery)  18.5 us
    all_to_all x2, starting transfers between devices, relay_weights(): lax.all_to_all(gate_rows, FS, split_axis=1, concat_axis=0, tiled=True)  17 us
    ppermute x4, waiting for transfers between devices, arrange_the_seats_all(): lax.ppermute(earlier[-1] if earlier else xin, axis_name=which_axis, perm=...  16.5 us
  transfers between devices with their start and end apart: 15, of which 12 were waited for; matrix products, arithmetic and copies ran while one was open for 5% of the time, Pallas kernels for 0%

profile of v1, /device:TPU:34, one launch (start us, length us, event | category | flops | bytes accessed | tf_op | source)
XLA Modules:
  0.0 537.8 jit_solution(1482552838130556016)
XLA Ops:
  7.2 1.0 convert_element_type.62
  8.2 1.7 collective-permute-start
  9.9 17.9 %collective-permute-start.2 = (bf16[64,1408]{1,0:T(8,128)(2,1)S(1)}, bf16[64,1408]{1,0:T(8,128)(2,1)S(1)}, u32[]{:S(2)}, u32[]{:S(2)}) collective-permute-start(bf16[64,1408]{1,0:T(8,128)(2,1)S(1)} %convert_element_type.62), channel_id=1, source_target_pairs={{1,0},{2,1},{3,2},{0,3},{5,4},{6,5},{7,6},{4,7},{9,8},{10,9},{11,1... | collective-permute-start | bytes 540680 | tf_op jit(solution)/shard_map/ppermute | solution.py:31
  27.8 1.0 convert_bitcast_fusion
  28.8 2.3 collective-permute-done
  31.2 6.6 %collective-permute-done.1 = bf16[64,1408]{1,0:T(8,128)(2,1)S(1)} collective-permute-done((bf16[64,1408]{1,0:T(8,128)(2,1)S(1)}, bf16[64,1408]{1,0:T(8,128)(2,1)S(1)}, u32[]{:S(2)}, u32[]{:S(2)}) %collective-permute-start.1) | collective-permute-done | bytes 180256 | tf_op jit(solution)/shard_map/ppermute | solution.py:26
  37.9 0.1 pad_maximum_fusion
  38.0 0.7 gather_fusion
  38.7 0.6 copy.31
  39.2 1.5 all_to_all.56
  40.8 1.6 copy.32
  42.3 7.4 %all-to-all-start = ((bf16[64,32,176]{2,0,1:T(8,128)(2,1)}), bf16[64,32,176]{2,0,1:T(8,128)(2,1)S(1)}, u32[]{:S(2)}, u32[]{:S(2)}) async-start(bf16[64,32,176]{2,0,1:T(8,128)(2,1)} %copy.32), calls=%async_computation | async-start | bytes 2097152 | tf_op jit(solution)/shard_map/all_to_all | solution.py:78
  49.8 13.9 %all_gather.15 = bf16[64,5632]{1,0:T(8,128)(2,1)S(1)} all-gather(bf16[64,1408]{1,0:T(8,128)(2,1)S(1)} %convert_element_type.63), channel_id=1, replica_groups=mesh['grp'=2,'fs_0'=16,'fs_1'=2,'tp'=4] {'tp'}, dimensions={1}, use_global_device_ids=true | all-gather | bytes 901120 | tf_op jit(solution)/shard_map/all_gather | solution.py:74
  63.7 2.0 all_to_all.60
  65.7 1.6 copy.33
  67.3 37.7 %all-to-all-done = bf16[64,32,176]{2,0,1:T(8,128)(2,1)S(1)} async-done(((bf16[64,32,176]{2,0,1:T(8,128)(2,1)}), bf16[64,32,176]{2,0,1:T(8,128)(2,1)S(1)}, u32[]{:S(2)}, u32[]{:S(2)}) %all-to-all-start) | async-done | bytes 720928 | tf_op jit(solution)/shard_map/all_to_all | solution.py:78
  105.0 4.8 all-to-all-start.1
  110.0 13.7 %all_gather.16 = bf16[176,2048]{1,0:T(8,128)(2,1)S(1)} all-gather(bf16[176,512]{1,0:T(8,128)(2,1)S(1)} %convert_element_type.65), channel_id=1, replica_groups=mesh['grp'=2,'fs_0'=16,'fs_1'=2,'tp'=4] {'tp'}, dimensions={1}, use_global_device_ids=true | all-gather | bytes 901120 | tf_op jit(solution)/shard_map/all_gather | solution.py:75
  123.7 4.0 fusion.4
  127.7 37.9 %all-to-all-done.1 = bf16[64,32,176]{2,0,1:T(8,128)(2,1)S(1)} async-done(((bf16[64,32,176]{2,0,1:T(8,128)(2,1)}), bf16[64,32,176]{2,0,1:T(8,128)(2,1)S(1)}, u32[]{:S(2)}, u32[]{:S(2)}) %all-to-all-start.1) | async-done | bytes 720928 | tf_op jit(solution)/shard_map/all_to_all | solution.py:79
  165.6 7.0 %convolution_convert_fusion.1 = bf16[1024,2048]{1,0:T(8,128)(2,1)} fusion(bf16[176,2048]{1,0:T(8,128)(2,1)S(1)} %all_gather.16, bf16[2048,176]{1,0:T(8,128)(2,1)S(1)} %bitcast.74, bf16[1,1024,2048]{2,1,0:T(8,128)(2,1)} %param.8, f32[1024,176]{0,1:T(8,128)S(1)} %fusion.4), kind=kOutput, calls=%fused_computation.7 | convolution fusion | flops 1479573504 | bytes 10551296 | tf_op jit(solution)/shard_map/dot_general | solution.py:85
  172.5 4.7 copy.34
  177.3 0.1 reduce-scatter.7.cloned.1.call-start
  177.4 12.8 %reduce-scatter.5.cloned.1.call-done = bf16[16,32,2048]{2,1,0:T(8,128)(2,1)} async-done(((bf16[32,32,2048]{2,1,0:T(8,128)(2,1)}), bf16[16,32,2048]{2,1,0:T(8,128)(2,1)}) %reduce-scatter.5.cloned.1.call-update) | async-done | bytes 2097168 | tf_op jit(solution)/shard_map/reduce_scatter | solution.py:44
  190.3 76.1 %reduce-scatter.7.cloned.1.call-done = bf16[1,32,2048]{2,1,0:T(8,128)(2,1)} async-done(((bf16[16,32,2048]{2,1,0:T(8,128)(2,1)}), bf16[1,32,2048]{2,1,0:T(8,128)(2,1)}) %reduce-scatter.7.cloned.1.call-update) | async-done | bytes 131088 | tf_op jit(solution)/shard_map/reduce_scatter | solution.py:44
  266.4 1.1 fusion.29
  267.6 1.2 multiply_reduce_fusion.1
  268.8 1.7 multiply_convert_fusion.3
  270.6 0.1 dynamic_slice.7
  270.6 0.8 multiply_convert_fusion.1
  271.4 1.4 collective-permute-start.3
  272.8 0.6 collective-permute-start.5
  273.5 3.5 collective-permute-done.3
  276.9 1.4 collective-permute-start.4
  278.3 4.1 collective-permute-done.4
  282.4 0.1 pad_maximum_fusion.1
  282.5 0.7 gather_fusion.1
  283.2 1.4 copy.35
  284.6 2.8 all_to_all.64
  287.4 1.6 copy.36
  289.0 9.7 %all-to-all-start.2 = ((bf16[64,32,176]{2,0,1:T(8,128)(2,1)}), bf16[64,32,176]{2,0,1:T(8,128)(2,1)S(1)}, u32[]{:S(2)}, u32[]{:S(2)}) async-start(bf16[64,32,176]{2,0,1:T(8,128)(2,1)} %copy.36), calls=%async_computation.4 | async-start | bytes 2097152 | tf_op jit(solution)/shard_map/all_to_all | solution.py:78
  298.6 14.5 %all_gather.18 = bf16[64,5632]{1,0:T(8,128)(2,1)} all-gather(bf16[64,1408]{1,0:T(8,128)(2,1)S(1)} %copy-done.5), channel_id=1, replica_groups=mesh['grp'=2,'fs_0'=16,'fs_1'=2,'tp'=4] {'tp'}, dimensions={1}, use_global_device_ids=true | all-gather | bytes 901120 | tf_op jit(solution)/shard_map/all_gather | solution.py:74
  313.1 3.8 all_to_all.68
  316.9 2.8 copy.37
  319.7 43.4 %all-to-all-done.2 = bf16[64,32,176]{2,0,1:T(8,128)(2,1)S(1)} async-done(((bf16[64,32,176]{2,0,1:T(8,128)(2,1)}), bf16[64,32,176]{2,0,1:T(8,128)(2,1)S(1)}, u32[]{:S(2)}, u32[]{:S(2)}) %all-to-all-start.2) | async-done | bytes 720928 | tf_op jit(solution)/shard_map/all_to_all | solution.py:78
  363.1 5.5 %all-to-all-start.3 = ((bf16[64,32,176]{2,0,1:T(8,128)(2,1)}), bf16[64,32,176]{2,0,1:T(8,128)(2,1)}, u32[]{:S(2)}, u32[]{:S(2)}) async-start(bf16[64,32,176]{2,0,1:T(8,128)(2,1)} %copy.37), calls=%async_computation.5 | async-start | bytes 2097152 | tf_op jit(solution)/shard_map/all_to_all | solution.py:79
  368.7 0.1 reduce-scatter.9.cloned.1.call-start
  368.8 14.7 %all_gather.19 = bf16[176,2048]{1,0:T(8,128)(2,1)} all-gather(bf16[176,512]{1,0:T(8,128)(2,1)S(1)} %convert_element_type.74), channel_id=1, replica_groups=mesh['grp'=2,'fs_0'=16,'fs_1'=2,'tp'=4] {'tp'}, dimensions={1}, use_global_device_ids=true | all-gather | bytes 901120 | tf_op jit(solution)/shard_map/all_gather | solution.py:75
  383.5 4.6 fusion.34
  388.1 36.0 %all-to-all-done.3 = bf16[64,32,176]{2,0,1:T(8,128)(2,1)} async-done(((bf16[64,32,176]{2,0,1:T(8,128)(2,1)}), bf16[64,32,176]{2,0,1:T(8,128)(2,1)}, u32[]{:S(2)}, u32[]{:S(2)}) %all-to-all-start.3) | async-done | bytes 720928 | tf_op jit(solution)/shard_map/all_to_all | solution.py:79
  424.1 7.7 %convolution_convert_fusion = bf16[1024,2048]{1,0:T(8,128)(2,1)} fusion(bf16[176,2048]{1,0:T(8,128)(2,1)} %all_gather.19, bf16[1024,2048]{1,0:T(8,128)(2,1)} %all-gather.2.cloned.1.call-done, bf16[2048,176]{1,0:T(8,128)(2,1)} %bitcast.24, f32[1024,176]{0,1:T(8,128)} %fusion.34), kind=kOutput, calls=%fused_computation.6 | convolution fusion | flops 1479573504 | bytes 10551296 | tf_op jit(solution)/shard_map/dot_general | solution.py:85
  431.7 4.7 copy.38
  436.5 0.1 reduce-scatter.11.cloned.1.call-start
  436.6 12.8 %reduce-scatter.9.cloned.1.call-done = bf16[16,32,2048]{2,1,0:T(8,128)(2,1)} async-done(((bf16[32,32,2048]{2,1,0:T(8,128)(2,1)}), bf16[16,32,2048]{2,1,0:T(8,128)(2,1)}) %reduce-scatter.9.cloned.1.call-update) | async-done | bytes 2097168 | tf_op jit(solution)/shard_map/reduce_scatter | solution.py:44
  449.5 2.2 copy.42
  451.7 1.2 copy.40
  452.9 1.2 copy.41
  454.1 1.2 copy.39
  455.3 70.1 %reduce-scatter.11.cloned.1.call-done = bf16[1,32,2048]{2,1,0:T(8,128)(2,1)} async-done(((bf16[16,32,2048]{2,1,0:T(8,128)(2,1)}), bf16[1,32,2048]{2,1,0:T(8,128)(2,1)}) %reduce-scatter.11.cloned.1.call-update) | async-done | bytes 131088 | tf_op jit(solution)/shard_map/reduce_scatter | solution.py:44
  525.5 1.1 fusion.28
  526.6 1.1 multiply_reduce_fusion
  527.7 1.8 multiply_convert_fusion.2
  529.5 0.9 copy.45
  530.4 0.9 copy.46
  (49 shorter events, 0.6 us)
Async XLA Ops:
  8.2 23.0 %collective-permute-start = (bf16[64,1408]{1,0:T(8,128)(2,1)S(1)}, bf16[64,1408]{1,0:T(8,128)(2,1)S(1)}, u32[]{:S(2)}, u32[]{:S(2)}) collective-permute-start(bf16[64,1408]{1,0:T(8,128)(2,1)S(1)} %convert_element_type.62), channel_id=1, source_target_pairs={{0,1},{1,2},{2,3},{3,0},{4,5},{5,6},{6,7},{7,4},{8,9},{9,10},{10,1... | collective-permute-start | bytes 540680 | tf_op jit(solution)/shard_map/ppermute | solution.py:26
  9.9 21.3 %collective-permute-start.2 = (bf16[64,1408]{1,0:T(8,128)(2,1)S(1)}, bf16[64,1408]{1,0:T(8,128)(2,1)S(1)}, u32[]{:S(2)}, u32[]{:S(2)}) collective-permute-start(bf16[64,1408]{1,0:T(8,128)(2,1)S(1)} %convert_element_type.62), channel_id=1, source_target_pairs={{1,0},{2,1},{3,2},{0,3},{5,4},{6,5},{7,6},{4,7},{9,8},{10,9},{11,1... | collective-permute-start | bytes 540680 | tf_op jit(solution)/shard_map/ppermute | solution.py:31
  31.2 6.7 %collective-permute-start.1 = (bf16[64,1408]{1,0:T(8,128)(2,1)S(1)}, bf16[64,1408]{1,0:T(8,128)(2,1)S(1)}, u32[]{:S(2)}, u32[]{:S(2)}) collective-permute-start(bf16[64,1408]{1,0:T(8,128)(2,1)S(1)} %collective-permute-done), channel_id=1, source_target_pairs={{0,1},{1,2},{2,3},{3,0},{4,5},{5,6},{6,7},{7,4},{8,9},{9,10},{10,1... | collective-permute-start | bytes 540680 | tf_op jit(solution)/shard_map/ppermute | solution.py:26
  38.0 11.7 %copy-start.6 = (f32[64,1408]{1,0:T(8,128)S(1)}, f32[64,1408]{1,0:T(8,128)}, u32[]{:S(2)}) copy-start(f32[64,1408]{1,0:T(8,128)} %param.10) | copy-start | bytes 1081348
  42.3 62.7 %all-to-all-start = ((bf16[64,32,176]{2,0,1:T(8,128)(2,1)}), bf16[64,32,176]{2,0,1:T(8,128)(2,1)S(1)}, u32[]{:S(2)}, u32[]{:S(2)}) async-start(bf16[64,32,176]{2,0,1:T(8,128)(2,1)} %copy.32), calls=%async_computation | async-start | bytes 2097152 | tf_op jit(solution)/shard_map/all_to_all | solution.py:78
  49.7 60.2 %copy-start.7 = (f32[176,512]{1,0:T(8,128)S(1)}, f32[176,512]{1,0:T(8,128)}, u32[]{:S(2)}) copy-start(f32[176,512]{1,0:T(8,128)} %param.11) | copy-start | bytes 1081348
  105.0 60.6 %all-to-all-start.1 = ((bf16[64,32,176]{2,0,1:T(8,128)(2,1)}), bf16[64,32,176]{2,0,1:T(8,128)(2,1)S(1)}, u32[]{:S(2)}, u32[]{:S(2)}) async-start(bf16[64,32,176]{2,0,1:T(8,128)(2,1)} %copy.33), calls=%async_computation.1 | async-start | bytes 2097152 | tf_op jit(solution)/shard_map/all_to_all | solution.py:79
  109.9 80.3 %reduce-scatter.5.cloned.1.call-start = ((), (), s32[]{:S(2)}) async-start(), calls=%async_computation.8 | async-start | bytes 6291456 | tf_op jit(solution)/shard_map/reduce_scatter | solution.py:44
  123.7 48.8 %copy-start = (bf16[176,2048]{1,0:T(8,128)(2,1)}, bf16[176,2048]{1,0:T(8,128)(2,1)S(1)}, u32[]{:S(2)}) copy-start(bf16[176,2048]{1,0:T(8,128)(2,1)S(1)} %all_gather.16) | copy-start | bytes 2162692
  177.3 93.3 %copy-start.11 = (f32[2048]{0:T(1024)S(1)}, f32[2048]{0:T(1024)}, u32[]{:S(2)}) copy-start(f32[2048]{0:T(1024)} %param.12) | copy-start | bytes 24580
  177.3 93.4 %copy-start.9 = (f32[64,1408]{1,0:T(8,128)S(1)}, f32[64,1408]{1,0:T(8,128)}, u32[]{:S(2)}) copy-start(f32[64,1408]{1,0:T(8,128)} %param.13) | copy-start | bytes 1081348
  177.3 93.4 %copy-start.10 = (f32[64,1408]{1,0:T(8,128)S(1)}, f32[64,1408]{1,0:T(8,128)}, u32[]{:S(2)}) copy-start(f32[64,1408]{1,0:T(8,128)} %param.14) | copy-start | bytes 1081348
  177.3 89.1 %reduce-scatter.7.cloned.1.call-start = ((), (), s32[]{:S(2)}) async-start(), calls=%async_computation.9 | async-start | bytes 2228224 | tf_op jit(solution)/shard_map/reduce_scatter | solution.py:44
  190.2 193.2 %all-gather.2.cloned.1.call-start = ((), (), s32[]{:S(2)}) async-start(), calls=%async_computation.10 | async-start | bytes 4325376 | tf_op jit(solution)/shard_map/all_gather | solution.py:113
  268.8 13.7 %copy-start.12 = (f32[32]{0:T(128)}, f32[32]{0:T(128)S(1)}, u32[]{:S(2)}) copy-start(f32[32]{0:T(128)S(1)} %add_rsqrt_fusion.1) | copy-start | bytes 388
  271.4 5.5 %collective-permute-start.3 = (bf16[64,1408]{1,0:T(8,128)(2,1)S(1)}, bf16[64,1408]{1,0:T(8,128)(2,1)S(1)}, u32[]{:S(2)}, u32[]{:S(2)}) collective-permute-start(bf16[64,1408]{1,0:T(8,128)(2,1)S(1)} %get-tuple-element.21), channel_id=1, source_target_pairs={{0,1},{1,2},{2,3},{3,0},{4,5},{5,6},{6,7},{7,4},{8,9},{9,10},{10,1... | collective-permute-start | bytes 540680 | tf_op jit(solution)/shard_map/ppermute | solution.py:26
  272.8 5.5 %collective-permute-start.5 = (bf16[64,1408]{1,0:T(8,128)(2,1)S(1)}, bf16[64,1408]{1,0:T(8,128)(2,1)S(1)}, u32[]{:S(2)}, u32[]{:S(2)}) collective-permute-start(bf16[64,1408]{1,0:T(8,128)(2,1)S(1)} %get-tuple-element.21), channel_id=1, source_target_pairs={{1,0},{2,1},{3,2},{0,3},{5,4},{6,5},{7,6},{4,7},{9,8},{10,9},{11,1... | collective-permute-start | bytes 540680 | tf_op jit(solution)/shard_map/ppermute | solution.py:31
  276.9 5.5 %collective-permute-start.4 = (bf16[64,1408]{1,0:T(8,128)(2,1)S(1)}, bf16[64,1408]{1,0:T(8,128)(2,1)S(1)}, u32[]{:S(2)}, u32[]{:S(2)}) collective-permute-start(bf16[64,1408]{1,0:T(8,128)(2,1)S(1)} %collective-permute-done.3), channel_id=1, source_target_pairs={{0,1},{1,2},{2,3},{3,0},{4,5},{5,6},{6,7},{7,4},{8,9},{9,10},{10,1... | collective-permute-start | bytes 540680 | tf_op jit(solution)/shard_map/ppermute | solution.py:26
  284.6 14.0 %copy-start.5 = (bf16[64,1408]{1,0:T(8,128)(2,1)S(1)}, bf16[64,1408]{1,0:T(8,128)(2,1)}, u32[]{:S(2)}) copy-start(bf16[64,1408]{1,0:T(8,128)(2,1)} %get-tuple-element.22) | copy-start | bytes 540676
  289.0 74.2 %all-to-all-start.2 = ((bf16[64,32,176]{2,0,1:T(8,128)(2,1)}), bf16[64,32,176]{2,0,1:T(8,128)(2,1)S(1)}, u32[]{:S(2)}, u32[]{:S(2)}) async-start(bf16[64,32,176]{2,0,1:T(8,128)(2,1)} %copy.36), calls=%async_computation.4 | async-start | bytes 2097152 | tf_op jit(solution)/shard_map/all_to_all | solution.py:78
  313.1 55.6 %copy-start.8 = (f32[176,512]{1,0:T(8,128)S(1)}, f32[176,512]{1,0:T(8,128)}, u32[]{:S(2)}) copy-start(f32[176,512]{1,0:T(8,128)} %param.15) | copy-start | bytes 1081348
  363.1 60.9 %all-to-all-start.3 = ((bf16[64,32,176]{2,0,1:T(8,128)(2,1)}), bf16[64,32,176]{2,0,1:T(8,128)(2,1)}, u32[]{:S(2)}, u32[]{:S(2)}) async-start(bf16[64,32,176]{2,0,1:T(8,128)(2,1)} %copy.37), calls=%async_computation.5 | async-start | bytes 2097152 | tf_op jit(solution)/shard_map/all_to_all | solution.py:79
  368.7 80.7 %reduce-scatter.9.cloned.1.call-start = ((), (), s32[]{:S(2)}) async-start(), calls=%async_computation.11 | async-start | bytes 6291456 | tf_op jit(solution)/shard_map/reduce_scatter | solution.py:44
  436.5 89.0 %reduce-scatter.11.cloned.1.call-start = ((), (), s32[]{:S(2)}) async-start(), calls=%async_computation.12 | async-start | bytes 2228224 | tf_op jit(solution)/shard_map/reduce_scatter | solution.py:44
  449.4 76.1 %copy-start.4 = (bf16[32,2048]{1,0:T(8,128)(2,1)S(1)}, bf16[32,2048]{1,0:T(8,128)(2,1)}, u32[]{:S(2)}) copy-start(bf16[32,2048]{1,0:T(8,128)(2,1)} %multiply_convert_fusion.3) | copy-start | bytes 393220
  449.5 78.2 %copy-start.3 = (bf16[1,32,2048]{2,1,0:T(8,128)(2,1)S(1)}, bf16[1,32,2048]{2,1,0:T(8,128)(2,1)}, u32[]{:S(2)}) copy-start(bf16[1,32,2048]{2,1,0:T(8,128)(2,1)} %reduce-scatter.7.cloned.1.call-done) | copy-start | bytes 393220
  449.5 78.2 %copy-start.13 = (f32[32]{0:T(128)S(1)}, f32[32]{0:T(128)}, u32[]{:S(2)}) copy-start(f32[32]{0:T(128)} %copy-done.12) | copy-start | bytes 388
  452.9 76.6 %copy-start.1 = (bf16[176,2048]{1,0:T(8,128)(2,1)S(1)}, bf16[176,2048]{1,0:T(8,128)(2,1)}, u32[]{:S(2)}) copy-start(bf16[176,2048]{1,0:T(8,128)(2,1)} %copy-done) | copy-start | bytes 2162692
  454.1 76.2 %copy-start.2 = (bf16[176,2048]{1,0:T(8,128)(2,1)S(1)}, bf16[176,2048]{1,0:T(8,128)(2,1)}, u32[]{:S(2)}) copy-start(bf16[176,2048]{1,0:T(8,128)(2,1)} %all_gather.19) | copy-start | bytes 2162692
Sparse Core Ops, SparseCore 0:
  177.5 12.6 reduce-scatter.4
  192.7 73.6 reduce-scatter.6
  270.7 98.1 all-gather.1
  436.6 12.7 reduce-scatter.8
  451.8 73.6 reduce-scatter.10
